TPU v7x, 32 devices: a whole 2x2x4 slice. The times are simulated.
32 devices in a mesh: grp: 2 (over y), sp: 4 (over z), tp: 4 (over x, core).
Axes of the slice: x: 2, y: 2, z: 4, core: 2. Of those that a mesh axis runs over, the one named last changes fastest.
Arguments:
- tokens: bfloat16 [4096, 2048], P(('grp', 'sp')), parts along dimension 0, may hold values from -6 to 6
- fresh_token_input: bfloat16 [4096], P('grp'), parts along dimension 0, may hold values from -6 to 6
- value_matrix: bfloat16 [2048, 2048], P(None, 'tp'), may hold values from -0.125 to 0.125
- write_matrix: bfloat16 [2048, 1024], P(None, 'tp'), may hold values from -0.125 to 0.125
- read_matrix: bfloat16 [2048, 1024], P(None, 'tp'), may hold values from -0.125 to 0.125
- gate_matrix: bfloat16 [2048, 2048], P(None, 'tp'), may hold values from -0.125 to 0.125
- step_matrix: bfloat16 [2048, 32], replicated, may hold values from -0.125 to 0.125
- value_filter_taps: bfloat16 [4, 2048], replicated, may hold values from -3 to 3
- write_filter_taps: bfloat16 [4, 1024], replicated, may hold values from -3 to 3
- read_filter_taps: bfloat16 [4, 1024], replicated, may hold values from -3 to 3
- head_log_decay: float32 [32], replicated
- step_offset_bias: float32 [32], replicated, may hold values from -3.5 to -2.5
- decay_spike: float32 [4096, 32], P(('grp', 'sp'), 'tp'), parts along dimension 0, may hold values from -3 to 0, as said below
- bypass_scale: float32 [32], replicated, may hold values from 0.5 to 2
- group_norm_scale: float32 [2048], replicated, may hold values from 0.1 to 1.9
Outputs:
- prompt_out: bfloat16 [4096, 2048], P(('grp', 'sp'), 'tp'), parts along dimension 0
- state_cache: bfloat16 [256, 2048], P(('grp', 'sp'), 'tp'), parts along dimension 0
- step_out: bfloat16 [1024, 4], P(('grp', 'tp'), 'sp'), parts along dimension 0
There are 2 independent parts, one for each index of `grp`. A program takes and returns all parts, laid end to end along the dimension named above; an argument that names none is the same for every part. Nothing has to cross between parts.
Inputs may be any that keep to these rules, and one draw needn't show every extreme that they name: `decay_spike`: never positive.
All inputs are finite; a program needn't handle non-finite values.
Results may differ from a plain program's by a relative error of at most 0.023.
Values may be sent and summed in bfloat16 or wider, within the bound.
A program may use at most 64 MiB of HBM per device.

v0:
```python
import jax
import jax.numpy as jnp
from jax import lax
from jax.sharding import PartitionSpec as P

HEAD = 64
STATE = 128
CONV = 4
BLOCK = 128
epsilon = 1e-06


def passed_along(block, axis, distance):
    devices = range(lax.axis_size(axis))
    route = [(i - distance, i) for i in devices if i - distance in devices]
    return lax.ppermute(block, axis, route)


def from_root(value, axis, source):
    kept = jnp.where(lax.axis_index(axis) == source, value, 0).astype(value.dtype)
    return lax.psum(kept, axis)


def project(operand, weights):
    return jnp.dot(operand, weights, preferred_element_type=jnp.float32).astype(jnp.bfloat16)


def apply_taps(previous, current, tap_weights):
    joined = jnp.concatenate([previous, current], axis=0).astype(jnp.float32)
    length = current.shape[0]
    summed = jnp.zeros(current.shape, jnp.float32)
    for offset in range(CONV):
        summed = summed + tap_weights[offset].astype(jnp.float32) * joined[offset : offset + length]
    return summed


def group_norm(gated_rows, groups):
    shaped = gated_rows.reshape(gated_rows.shape[:-1] + (groups, -1))
    normed = shaped * lax.rsqrt(jnp.mean(shaped * shaped, axis=-1, keepdims=True) + epsilon)
    return normed.reshape(gated_rows.shape)


def read_new(cached, stored_portion, read_part, new_decay, step_now, value_now):
    states = cached.astype(jnp.float32).reshape((cached.shape[0],) + value_now.shape)
    updated = (
        new_decay[None, :, :, None] * states
        + step_now[None, :, :, None] * stored_portion.T[:, :, None, None] * value_now[None]
    )
    return jnp.einsum("gn,ngep->gep", read_part, updated, precision=lax.Precision.HIGHEST)


def on_device(
    tokens,
    fresh_token_input,
    value_matrix,
    write_matrix,
    read_matrix,
    gate_matrix,
    step_matrix,
    value_filter_taps,
    write_filter_taps,
    read_filter_taps,
    head_log_decay,
    step_offset_bias,
    decay_spike,
    bypass_scale,
    group_norm_scale,
):
    head_rank = lax.axis_index("tp")
    sequence_rank = lax.axis_index("sp")
    sequence_count = lax.axis_size("sp")
    channels = value_matrix.shape[1]
    head_count = channels // HEAD
    map_width = write_matrix.shape[1]
    group_count = map_width // STATE
    per_group = head_count // group_count
    row_count = tokens.shape[0]
    head_start = head_rank * head_count
    local_count = STATE // sequence_count
    own_step = lax.dynamic_slice_in_dim(step_matrix, head_start, head_count, 1)
    own_value_taps = lax.dynamic_slice_in_dim(value_filter_taps, head_rank * channels, channels, 1)
    own_write_taps = lax.dynamic_slice_in_dim(
        write_filter_taps, head_rank * map_width, map_width, 1
    )
    own_read_taps = lax.dynamic_slice_in_dim(read_filter_taps, head_rank * map_width, map_width, 1)
    head_decay_rates = jnp.exp(lax.dynamic_slice_in_dim(head_log_decay, head_start, head_count, 0))
    own_bias = lax.dynamic_slice_in_dim(step_offset_bias, head_start, head_count, 0)
    own_skip = lax.dynamic_slice_in_dim(bypass_scale, head_start, head_count, 0)
    own_gain = lax.dynamic_slice_in_dim(group_norm_scale, head_rank * channels, channels, 0)
    value_rows = project(tokens, value_matrix)
    write_rows = project(tokens, write_matrix)
    read_rows = project(tokens, read_matrix)
    gate_rows = project(tokens, gate_matrix)
    step_raw = jnp.dot(tokens, own_step, preferred_element_type=jnp.float32)
    edge = row_count - (CONV - 1)
    tail_rows = (value_rows[edge:], write_rows[edge:], read_rows[edge:])
    before = passed_along((tail_rows[0], tail_rows[1], tail_rows[2]), "sp", 1)
    ending = (
        from_root(tail_rows[0], "sp", sequence_count - 1),
        from_root(tail_rows[1], "sp", sequence_count - 1),
        from_root(tail_rows[2], "sp", sequence_count - 1),
    )
    values = jax.nn.silu(apply_taps(before[0], value_rows, own_value_taps)).astype(jnp.bfloat16)
    writes = jax.nn.silu(apply_taps(before[1], write_rows, own_write_taps)).astype(jnp.bfloat16)
    reads = jax.nn.silu(apply_taps(before[2], read_rows, own_read_taps)).astype(jnp.bfloat16)
    step_length = jax.nn.softplus(step_raw + own_bias)
    log_decay_value = decay_spike - step_length * head_decay_rates
    blocks = row_count // BLOCK
    block_values = values.reshape(blocks, BLOCK, group_count, per_group, HEAD)
    block_writes = writes.reshape(blocks, BLOCK, group_count, STATE)
    block_reads = reads.reshape(blocks, BLOCK, group_count, STATE)
    block_steps = step_length.reshape(blocks, BLOCK, group_count, per_group)
    cumulative = jnp.cumsum(log_decay_value.reshape(blocks, BLOCK, group_count, per_group), axis=1)
    block_end = cumulative[:, -1]
    scaled = (
        (jnp.exp(block_end[:, None] - cumulative) * block_steps)[..., None]
        * block_values.astype(jnp.float32)
    ).astype(jnp.bfloat16)
    block_states = jnp.einsum(
        "bsgn,bsgep->bngep", block_writes, scaled, preferred_element_type=jnp.float32
    )
    running = jnp.zeros((STATE, group_count, per_group, HEAD), jnp.float32)
    inside = []
    for block_index in range(blocks):
        inside.append(running)
        running = (
            jnp.exp(block_end[block_index])[None, :, :, None] * running + block_states[block_index]
        )
    local_states = jnp.stack(inside)
    shard_fading_factor = jnp.sum(block_end, axis=0)
    before_block = jnp.cumsum(block_end, axis=0) - block_end
    decay_table = lax.all_gather(shard_fading_factor[None], "sp", axis=0, tiled=True)
    inclusive = jnp.cumsum(decay_table, axis=0)
    exclusive = inclusive - decay_table
    total_decay = inclusive[-1]
    row_pieces = lax.all_to_all(running[None], "sp", split_axis=1, concat_axis=0, tiled=True)
    ranks = jnp.arange(sequence_count)
    below = (ranks[None, :] < ranks[:, None])[:, :, None, None]
    prefix_weight = jnp.exp(jnp.where(below, exclusive[:, None] - inclusive[None, :], -jnp.inf))
    prefix_rows = jnp.einsum(
        "jkge,kngep->jngep", prefix_weight, row_pieces, precision=lax.Precision.HIGHEST
    )
    final_weight = jnp.exp(total_decay[None] - inclusive)
    final_rows = jnp.einsum(
        "kge,kngep->ngep", final_weight, row_pieces, precision=lax.Precision.HIGHEST
    )
    earlier_state = lax.all_to_all(prefix_rows, "sp", split_axis=0, concat_axis=1, tiled=True)[0]
    scores = jnp.einsum(
        "blgn,bsgn->bgls", block_reads, block_writes, preferred_element_type=jnp.float32
    )
    cum_heads = jnp.transpose(cumulative, (0, 2, 3, 1))
    decay_gaps = cum_heads[..., :, None] - cum_heads[..., None, :]
    step_heads = jnp.transpose(block_steps, (0, 2, 3, 1))
    causal = jnp.tril(jnp.ones((BLOCK, BLOCK), bool))
    mixing = (
        scores[:, :, None]
        * jnp.exp(jnp.where(causal, decay_gaps, -jnp.inf))
        * step_heads[..., None, :]
    ).astype(jnp.bfloat16)
    inner_part = jnp.einsum(
        "bgels,bsgep->blgep", mixing, block_values, preferred_element_type=jnp.float32
    )
    entering = jnp.exp(before_block)[:, None, :, :, None] * earlier_state[None] + local_states
    carried_part = jnp.exp(cumulative)[..., None] * jnp.einsum(
        "blgn,bngep->blgep",
        block_reads.astype(jnp.float32),
        entering,
        precision=lax.Precision.HIGHEST,
    )
    mixed_rows = (inner_part + carried_part).reshape(row_count, head_count, HEAD) + own_skip[
        None, :, None
    ] * values.astype(jnp.float32).reshape(row_count, head_count, HEAD)
    gated_rows = mixed_rows.reshape(row_count, channels) * jax.nn.silu(
        gate_rows.astype(jnp.float32)
    )
    prompt_out = (group_norm(gated_rows, group_count) * own_gain).astype(jnp.bfloat16)
    new_row = fresh_token_input[None]
    new_value = project(new_row, value_matrix)
    new_write = project(new_row, write_matrix)
    new_read = project(new_row, read_matrix)
    new_gate = project(new_row, gate_matrix)
    new_step = jax.nn.softplus(
        jnp.dot(new_row, own_step, preferred_element_type=jnp.float32)[0] + own_bias
    )
    new_values = jax.nn.silu(apply_taps(ending[0], new_value, own_value_taps)).astype(jnp.bfloat16)
    latest_stores = jax.nn.silu(apply_taps(ending[1], new_write, own_write_taps)).astype(
        jnp.bfloat16
    )
    new_reads = jax.nn.silu(apply_taps(ending[2], new_read, own_read_taps)).astype(jnp.bfloat16)
    value_now = new_values.astype(jnp.float32).reshape(group_count, per_group, HEAD)
    write_now = latest_stores.astype(jnp.float32).reshape(group_count, STATE)
    read_now = new_reads.astype(jnp.float32).reshape(group_count, STATE)
    new_decay = jnp.exp(-new_step * head_decay_rates).reshape(group_count, per_group)
    step_now = new_step.reshape(group_count, per_group)
    row_start = sequence_rank * local_count
    cache_rows = final_rows.reshape(local_count, channels).astype(jnp.bfloat16)
    stored_portion = lax.dynamic_slice_in_dim(write_now, row_start, local_count, 1)
    read_part = lax.dynamic_slice_in_dim(read_now, row_start, local_count, 1)
    partial_value = read_new(cache_rows, stored_portion, read_part, new_decay, step_now, value_now)
    reading = lax.psum(partial_value, "sp")
    new_mixed = reading + own_skip.reshape(group_count, per_group)[:, :, None] * value_now
    new_gated = new_mixed.reshape(1, channels) * jax.nn.silu(new_gate.astype(jnp.float32))
    step_whole = (group_norm(new_gated, group_count) * own_gain).astype(jnp.bfloat16)[0]
    step_table = step_whole.reshape(channels // sequence_count, sequence_count)
    step_out = lax.dynamic_slice_in_dim(step_table, sequence_rank, 1, 1)
    return (prompt_out, cache_rows, step_out)


def solution(mesh):
    placed = (
        P(("grp", "sp"), None),
        P("grp"),
        P(None, "tp"),
        P(None, "tp"),
        P(None, "tp"),
        P(None, "tp"),
        P(),
        P(),
        P(),
        P(),
        P(),
        P(),
        P(("grp", "sp"), "tp"),
        P(),
        P(),
    )
    return jax.shard_map(
        on_device,
        mesh=mesh,
        in_specs=placed,
        out_specs=(P(("grp", "sp"), "tp"), P(("grp", "sp"), "tp"), P(("grp", "tp"), "sp")),
        check_vma=False,
    )
```

profile of v0, /device:TPU:0, one launch (start us, length us, event | category | flops | bytes accessed | tf_op | source)
XLA Modules:
  0.0 126.4 jit_solution(4960432107386798171)
XLA Ops:
  0.7 1.6 %copy-done = bf16[512,2048]{1,0:T(8,128)(2,1)S(1)} copy-done((bf16[512,2048]{1,0:T(8,128)(2,1)S(1)}, bf16[512,2048]{1,0:T(8,128)(2,1)}, u32[]{:S(2)}) %copy-start) | copy-done | bytes 2097176
  2.2 1.9 %convolution_convert_fusion.2 = bf16[512,256]{1,0:T(8,128)(2,1)S(1)} fusion(bf16[512,2048]{1,0:T(8,128)(2,1)S(1)} %copy-done, bf16[2048,256]{1,0:T(8,128)(2,1)} %param.18), kind=kOutput, calls=%fused_computation.11 | convolution fusion | flops 537001984 | bytes 3407872 | tf_op jit(solution)/shard_map/dot_general | solution.py:25
  4.7 5.7 %collective-permute-start.2 = (bf16[3,256]{1,0:T(4,128)(2,1)}, bf16[3,256]{1,0:T(4,128)(2,1)}, u32[]{:S(2)}, u32[]{:S(2)}) collective-permute-start(bf16[3,256]{1,0:T(4,128)(2,1)} %get-tuple-element.57), channel_id=1, source_target_pairs={{0,4},{4,8},{8,12},{1,5},{5,9},{9,13},{2,6},{6,10},{10,14},{3,7},{... | collective-permute-start | bytes 4616 | tf_op jit(solution)/shard_map/ppermute | solution.py:16
  11.8 3.6 %collective-permute-start.1 = (bf16[3,256]{1,0:T(4,128)(2,1)}, bf16[3,256]{1,0:T(4,128)(2,1)}, u32[]{:S(2)}, u32[]{:S(2)}) collective-permute-start(bf16[3,256]{1,0:T(4,128)(2,1)} %get-tuple-element.54), channel_id=1, source_target_pairs={{0,4},{4,8},{8,12},{1,5},{5,9},{9,13},{2,6},{6,10},{10,14},{3,7},{... | collective-permute-start | bytes 4616 | tf_op jit(solution)/shard_map/ppermute | solution.py:16
  15.4 1.3 convolution_convert_fusion.1
  18.1 3.5 %collective-permute-start = (bf16[3,512]{1,0:T(4,128)(2,1)}, bf16[3,512]{1,0:T(4,128)(2,1)}, u32[]{:S(2)}, u32[]{:S(2)}) collective-permute-start(bf16[3,512]{1,0:T(4,128)(2,1)} %get-tuple-element.52), channel_id=1, source_target_pairs={{0,4},{4,8},{8,12},{1,5},{5,9},{9,13},{2,6},{6,10},{10,14},{3,7},{... | collective-permute-start | bytes 9224 | tf_op jit(solution)/shard_map/ppermute | solution.py:16
  22.4 1.5 %fusion.96 = f32[1,256]{1,0:T(1,128)S(1)} fusion(bf16[2048,1]{0,1:T(2,128)(2,1)S(1)} %reshape.251, bf16[2048,256]{1,0:T(8,128)(2,1)} %param.19), kind=kOutput, calls=%fused_computation.194 | convolution fusion | flops 1048576 | bytes 1053696 | tf_op jit(solution)/shard_map/dot_general | solution.py:25
  27.1 2.0 %fusion.99 = f32[1,512]{1,0:T(1,128)S(1)} fusion(bf16[2048,1]{0,1:T(2,128)(2,1)S(1)} %reshape.251, bf16[2048,512]{1,0:T(8,128)(2,1)} %param.20), kind=kOutput, calls=%fused_computation.197 | convolution fusion | flops 2097152 | bytes 2103296 | tf_op jit(solution)/shard_map/dot_general | solution.py:25
  29.1 7.6 %all-gather.1 = f32[4,2,4]{2,1,0:T(2,128)S(1)} all-gather(f32[1,2,4]{2,1,0:T(2,128)S(1)} %bitcast.152), channel_id=2, replica_groups=mesh['grp'=2,'sp'=4,'tp'=4] {'sp'}, dimensions={0}, use_global_device_ids=true | all-gather | bytes 160 | tf_op jit(solution)/shard_map/all_gather | solution.py:132
  36.7 10.5 %all-reduce = (bf16[3,512]{1,0:T(4,128)(2,1)S(1)}, bf16[3,256]{1,0:T(4,128)(2,1)S(1)}, bf16[3,256]{1,0:T(4,128)(2,1)S(1)}) all-reduce(bf16[3,512]{1,0:T(4,128)(2,1)S(1)} %get-tuple-element.53, bf16[3,256]{1,0:T(4,128)(2,1)S(1)} %get-tuple-element.56, ...), channel_id=1, replica_groups=mesh['grp'=2,'sp'=4,'tp'=4] {'sp'}, use_global_device_ids=true, to_apply=%region_7.8 | all-reduce | flops 3072 | bytes 12288 | tf_op jit(solution)/shard_map/psum | solution.py:21
  49.9 2.4 %fusion.90 = (f32[4,128,2,4]{3,2,1,0:T(2,128)}, f32[4,128,2,4]{3,2,1,0:T(2,128)S(1)}) fusion(f32[4,128,2,4]{3,2,1,0:T(2,128)S(1)} %fusion.94, f32[4,128,2,4]{3,2,1,0:T(2,128)} %copy.149, f32[4,2,4]{2,1,0:T(2,128)S(1)} %get-tuple-element.47), kind=kLoop, calls=%fused_computation.187 | loop fusion | flops 8192 | bytes 65664 | tf_op jit(solution)/shard_map/exp | solution.py:164
  55.9 1.3 %mul.529 = f32[2,4]{1,0:T(2,128)} reshape(f32[8]{0:T(128)} %get-tuple-element.28) | data formatting | bytes 64 | tf_op jit(solution)/shard_map/mul | solution.py:46
  57.6 1.3 %copy.148 = f32[4,128,2,4]{1,3,2,0:T(4,128)S(1)} copy(f32[4,128,2,4]{3,2,1,0:T(2,128)} %get-tuple-element.44) | data formatting | bytes 32768 | tf_op jit(solution)/shard_map/exp | solution.py:164
  63.6 1.3 %multiply_convert_fusion.4 = bf16[512,512]{1,0:T(8,128)(2,1)S(1)} fusion(f32[515,512]{1,0:T(8,128)S(1)} %maximum_convert_fusion, f32[512]{0:T(512)} %bitcast.141, f32[512]{0:T(512)} %bitcast.140, f32[512]{0:T(512)S(1)} %bitcast.139, f32[512]{0:T(512)S(1)} %bitcast.138), kind=kLoop, calls=%fused_computation.44 | loop fusion | flops 3145728 | bytes 4726784 | tf_op jit(solution)/shard_map/convert_element_type | solution.py:103
  66.0 2.0 %reshape.229 = bf16[4,128,2,4,64]{1,0,4,3,2:T(4,128)(2,1)} reshape(bf16[512,512]{0,1:T(8,128)(2,1)} %copy.140) | data formatting | bytes 1048576 | tf_op jit(solution)/shard_map/reshape | solution.py:109
  68.0 1.3 multiply_convert_fusion.3
  70.8 1.2 reshape.274
  72.0 3.6 %all-to-all-start = ((f32[4,1,16384]{2,1,0:T(1,128)}), f32[4,1,16384]{2,1,0:T(1,128)S(1)}, u32[]{:S(2)}, u32[]{:S(2)}) async-start(f32[4,1,16384]{2,1,0:T(1,128)} %reshape.274), calls=%async_computation | async-start | bytes 524288 | tf_op jit(solution)/shard_map/all_to_all | solution.py:136
  75.9 3.0 %convolution_bitcast_fusion.2 = f32[4,128,2,4,64]{1,4,3,2,0:T(8,128)} fusion(f32[4,2,4,128]{3,2,1,0:T(4,128)S(1)} %copy.146, f32[4,2,4,128]{3,2,1,0:T(4,128)S(1)} %copy.144, f32[4,2,128,128]{3,2,1,0:T(8,128)S(1)} %fusion.40, pred[128,128]{1,0:T(8,128)(4,1)S(1)} %iota_compare_fusion, bf16[4,128,2,4,64]{1,0,4,3,2:T(4,128)(2,1)} %reshape.229), kind=kOutput, calls=%fused_computation.5 | convolution fusion | flops 69730304 | bytes 2146304 | tf_op jit(solution)/shard_map/bgels,bsgep->blgep/dot_general | solution.py:160
  78.8 3.3 %all-to-all-done = f32[4,1,16384]{2,1,0:T(1,128)S(1)} async-done(((f32[4,1,16384]{2,1,0:T(1,128)}), f32[4,1,16384]{2,1,0:T(1,128)S(1)}, u32[]{:S(2)}, u32[]{:S(2)}) %all-to-all-start) | async-done | bytes 262176 | tf_op jit(solution)/shard_map/all_to_all | solution.py:136
  82.7 1.3 %reduce.9 = f32[4,16384]{1,0:T(4,128)S(1)} reduce(f32[4,1,16384]{2,1,0:T(1,128)S(1)} %all-to-all-done, f32[]{:T(128)} %broadcast.118), dimensions={1}, to_apply=%all_to_all.6.reduce_sub_computation | reduce | bytes 524292 | tf_op jit(solution)/shard_map/all_to_all | solution.py:136
  84.4 1.3 %fusion.35 = bf16[2,4,1,32,64]{4,2,3,1,0:T(2,128)(2,1)S(1)} fusion(f32[4,2,4,1,1]{0,3,4,2,1:T(1,128)S(1)} %copy.173, f32[4,32,2,4,64]{4,3,2,1,0:T(4,128)S(1)} %bitcast.123), kind=kOutput, calls=%fused_computation.69 | convolution fusion | flops 786432 | bytes 295040 | tf_op jit(solution)/shard_map/kge,kngep->ngep/dot_general | solution.py:144
  85.7 1.3 %convolution_bitcast_fusion.3 = f32[4,32,2,4,64]{4,0,1,3,2:T(4,128)S(1)} fusion(f32[4,32,2,4,64]{4,3,2,1,0:T(4,128)S(1)} %bitcast.124, f32[4,2,4]{0,2,1:T(4,128)S(1)} %copy.156, f32[4,2,4]{0,2,1:T(4,128)S(1)} %copy.155, pred[4,4]{1,0:T(4,128)(4,1)S(1)} %copy-done.30), kind=kOutput, calls=%fused_computation.10 | convolution fusion | flops 3145984 | bytes 524560 | tf_op jit(solution)/shard_map/jkge,kngep->jngep/dot_general | solution.py:140
  88.1 3.4 %all-to-all-start.1 = ((f32[4,1,16384]{2,1,0:T(1,128)}), f32[4,1,16384]{2,1,0:T(1,128)S(1)}, u32[]{:S(2)}, u32[]{:S(2)}) async-start(f32[4,1,16384]{2,1,0:T(1,128)} %reshape.276), calls=%async_computation.1 | async-start | bytes 524288 | tf_op jit(solution)/shard_map/all_to_all | solution.py:147
  91.9 12.2 %psum.31 = f32[2,4,64]{2,1,0:T(4,128)S(1)} all-reduce(f32[2,4,64]{2,1,0:T(4,128)S(1)} %bitcast.137), channel_id=1, replica_groups=mesh['grp'=2,'sp'=4,'tp'=4] {'sp'}, use_global_device_ids=true, to_apply=%region_8.9 | all-reduce | flops 512 | bytes 4096 | tf_op jit(solution)/shard_map/psum | solution.py:200
  106.9 1.3 %reduce.10 = f32[4,16384]{1,0:T(4,128)S(1)} reduce(f32[4,1,16384]{2,1,0:T(1,128)S(1)} %all-to-all-done.1, f32[]{:T(128)} %broadcast.118), dimensions={1}, to_apply=%all_to_all.8.reduce_sub_computation | reduce | bytes 524292 | tf_op jit(solution)/shard_map/all_to_all | solution.py:147
  109.4 2.3 %fusion.1 = f32[4,128,2,4,64]{1,4,3,2,0:T(8,128)S(1)} fusion(f32[4,128,2,4,64]{1,4,3,2,0:T(8,128)} %convolution_bitcast_fusion.2, f32[1,128,2,4,64]{1,4,3,2,0:T(8,128)} %get-tuple-element.41, f32[1,128,2,4,64]{1,4,3,2,0:T(8,128)} %get-tuple-element.42, f32[1,128,2,4,64]{1,4,3,2,0:T(8,128)} %get-tuple-element.43, f32[4]{0:T(128)S(1)} %copy-done.31, ...), kind=kOutput, calls=%fused_computation.4 | convolution fusion | flops 404488192 | bytes 3424400 | tf_op jit(solution)/shard_map/blgn,bngep->blgep/dot_general | solution.py:164
  111.7 1.8 %copy.184 = f32[4,128,2,4,64]{4,3,2,1,0:T(4,128)} copy(f32[4,128,2,4,64]{1,4,3,2,0:T(8,128)S(1)} %fusion.1) | data formatting | bytes 2097152 | tf_op jit(solution)/shard_map/reshape | solution.py:170
  113.5 3.5 %reshape.263 = f32[512,512]{1,0:T(8,128)} reshape(f32[4,128,2,4,64]{4,3,2,1,0:T(4,128)} %copy.184) | data formatting | bytes 2097152 | tf_op jit(solution)/shard_map/reshape | solution.py:170
  117.0 4.6 %fusion.93 = (f32[512,512]{1,0:T(8,128)}, f32[512,512]{1,0:T(8,128)}) fusion(bf16[512,2048]{1,0:T(8,128)(2,1)S(1)} %copy-done, bf16[2048,512]{1,0:T(8,128)(2,1)} %param.20, f32[512,512]{1,0:T(8,128)} %reshape.263, bf16[512,512]{1,0:T(8,128)(2,1)S(1)} %copy-done.2, f32[512]{0:T(512)S(1)} %copy-done.25), kind=kOutput, calls=%fused_computation.190 | convolution fusion | flops 1076625408 | bytes 7866368 | tf_op jit(solution)/shard_map/dot_general | solution.py:25
  121.7 1.9 %mul.516 = f32[512,2,256]{2,1,0:T(2,128)S(1)} reshape(f32[512,512]{1,0:T(8,128)} %get-tuple-element.63) | data formatting | bytes 2097152 | tf_op jit(solution)/shard_map/mul | solution.py:39
  125.4 1.1 multiply_convert_fusion.2
  (160 shorter events, 29.5 us)
Async XLA Ops:
  0.6 9.8 %copy-start.6 = (bf16[2048,256]{1,0:T(8,128)(2,1)S(1)}, bf16[2048,256]{1,0:T(8,128)(2,1)}, u32[]{:S(2)}) copy-start(bf16[2048,256]{1,0:T(8,128)(2,1)} %param.19) | copy-start | bytes 3145732
  4.2 11.3 %copy-start.3 = (bf16[2048,512]{1,0:T(8,128)(2,1)S(1)}, bf16[2048,512]{1,0:T(8,128)(2,1)}, u32[]{:S(2)}) copy-start(bf16[2048,512]{1,0:T(8,128)(2,1)} %param.17) | copy-start | bytes 6291460
  4.7 55.0 %collective-permute-start.2 = (bf16[3,256]{1,0:T(4,128)(2,1)}, bf16[3,256]{1,0:T(4,128)(2,1)}, u32[]{:S(2)}, u32[]{:S(2)}) collective-permute-start(bf16[3,256]{1,0:T(4,128)(2,1)} %get-tuple-element.57), channel_id=1, source_target_pairs={{0,4},{4,8},{8,12},{1,5},{5,9},{9,13},{2,6},{6,10},{10,14},{3,7},{... | collective-permute-start | bytes 4616 | tf_op jit(solution)/shard_map/ppermute | solution.py:16
  11.8 10.3 %copy-start.23 = (bf16[2048]{0:T(1024)(128)(2,1)S(1)}, bf16[2048]{0:T(1024)(128)(2,1)}, u32[]{:S(2)}) copy-start(bf16[2048]{0:T(1024)(128)(2,1)} %param.16) | copy-start | bytes 12292
  11.8 10.3 %copy-start.5 = (bf16[2048,256]{1,0:T(8,128)(2,1)S(1)}, bf16[2048,256]{1,0:T(8,128)(2,1)}, u32[]{:S(2)}) copy-start(bf16[2048,256]{1,0:T(8,128)(2,1)} %param.18) | copy-start | bytes 3145732
  11.8 49.6 %collective-permute-start.1 = (bf16[3,256]{1,0:T(4,128)(2,1)}, bf16[3,256]{1,0:T(4,128)(2,1)}, u32[]{:S(2)}, u32[]{:S(2)}) collective-permute-start(bf16[3,256]{1,0:T(4,128)(2,1)} %get-tuple-element.54), channel_id=1, source_target_pairs={{0,4},{4,8},{8,12},{1,5},{5,9},{9,13},{2,6},{6,10},{10,14},{3,7},{... | collective-permute-start | bytes 4616 | tf_op jit(solution)/shard_map/ppermute | solution.py:16
  18.1 44.7 %collective-permute-start = (bf16[3,512]{1,0:T(4,128)(2,1)}, bf16[3,512]{1,0:T(4,128)(2,1)}, u32[]{:S(2)}, u32[]{:S(2)}) collective-permute-start(bf16[3,512]{1,0:T(4,128)(2,1)} %get-tuple-element.52), channel_id=1, source_target_pairs={{0,4},{4,8},{8,12},{1,5},{5,9},{9,13},{2,6},{6,10},{10,14},{3,7},{... | collective-permute-start | bytes 9224 | tf_op jit(solution)/shard_map/ppermute | solution.py:16
  21.6 2.3 %copy-start.4 = (bf16[2048,512]{1,0:T(8,128)(2,1)S(1)}, bf16[2048,512]{1,0:T(8,128)(2,1)}, u32[]{:S(2)}) copy-start(bf16[2048,512]{1,0:T(8,128)(2,1)} %param.17) | copy-start | bytes 6291460
  22.1 2.2 %copy-start.33 = (f32[32]{0:T(128)S(1)}, f32[32]{0:T(128)}, u32[]{:S(2)}) copy-start(f32[32]{0:T(128)} %param.26) | copy-start | bytes 388
  22.2 2.3 %copy-start.32 = (f32[32]{0:T(128)S(1)}, f32[32]{0:T(128)}, u32[]{:S(2)}) copy-start(f32[32]{0:T(128)} %param.25) | copy-start | bytes 388
  22.2 3.0 %copy-start.12 = (f32[512,8]{0,1:T(8,128)S(1)}, f32[512,8]{0,1:T(8,128)}, u32[]{:S(2)}) copy-start(f32[512,8]{0,1:T(8,128)} %param.27) | copy-start | bytes 49156
  22.4 2.0 %copy-start.13 = (bf16[2048,32]{0,1:T(8,128)(2,1)S(1)}, bf16[2048,32]{0,1:T(8,128)(2,1)}, u32[]{:S(2)}) copy-start(bf16[2048,32]{0,1:T(8,128)(2,1)} %param.21) | copy-start | bytes 393220
  25.8 21.5 %copy-start.26 = (bf16[4,1024]{1,0:T(4,128)(2,1)S(1)}, bf16[4,1024]{1,0:T(4,128)(2,1)}, u32[]{:S(2)}) copy-start(bf16[4,1024]{1,0:T(4,128)(2,1)} %param.23) | copy-start | bytes 24580
  26.1 23.0 %copy-start.27 = (bf16[4,1024]{1,0:T(4,128)(2,1)S(1)}, bf16[4,1024]{1,0:T(4,128)(2,1)}, u32[]{:S(2)}) copy-start(bf16[4,1024]{1,0:T(4,128)(2,1)} %param.24) | copy-start | bytes 24580
  27.1 25.3 %copy-start.22 = (bf16[4,2048]{1,0:T(4,128)(2,1)S(1)}, bf16[4,2048]{1,0:T(4,128)(2,1)}, u32[]{:S(2)}) copy-start(bf16[4,2048]{1,0:T(4,128)(2,1)} %param.22) | copy-start | bytes 49156
  57.6 3.9 %copy-start.11 = (bf16[512,256]{1,0:T(8,128)(2,1)S(1)}, bf16[512,256]{1,0:T(8,128)(2,1)}, u32[]{:S(2)}) copy-start(bf16[512,256]{1,0:T(8,128)(2,1)} %copy-done.10) | copy-start | bytes 786436
  59.1 3.1 %copy-start.18 = (f32[1,256]{1,0:T(1,128)S(1)}, f32[1,256]{1,0:T(1,128)}, u32[]{:S(2)}) copy-start(f32[1,256]{1,0:T(1,128)} %get-tuple-element.24) | copy-start | bytes 3076
  59.1 3.2 %copy-start.19 = (f32[1,256]{1,0:T(1,128)S(1)}, f32[1,256]{1,0:T(1,128)}, u32[]{:S(2)}) copy-start(f32[1,256]{1,0:T(1,128)} %get-tuple-element.25) | copy-start | bytes 3076
  59.1 3.2 %copy-start.20 = (f32[1,256]{1,0:T(1,128)S(1)}, f32[1,256]{1,0:T(1,128)}, u32[]{:S(2)}) copy-start(f32[1,256]{1,0:T(1,128)} %get-tuple-element.26) | copy-start | bytes 3076
  59.1 3.2 %copy-start.21 = (f32[1,256]{1,0:T(1,128)S(1)}, f32[1,256]{1,0:T(1,128)}, u32[]{:S(2)}) copy-start(f32[1,256]{1,0:T(1,128)} %get-tuple-element.27) | copy-start | bytes 3076
  65.0 4.5 %copy-start.1 = (bf16[512,512]{1,0:T(8,128)(2,1)}, bf16[512,512]{1,0:T(8,128)(2,1)S(1)}, u32[]{:S(2)}) copy-start(bf16[512,512]{1,0:T(8,128)(2,1)S(1)} %multiply_convert_fusion.4) | copy-start | bytes 1572868
  66.0 3.5 %copy-start.14 = (f32[2,4]{1,0:T(2,128)S(1)}, f32[2,4]{1,0:T(2,128)}, u32[]{:S(2)}) copy-start(f32[2,4]{1,0:T(2,128)} %get-tuple-element.48) | copy-start | bytes 100
  66.0 3.5 %copy-start.15 = (f32[2,4]{1,0:T(2,128)S(1)}, f32[2,4]{1,0:T(2,128)}, u32[]{:S(2)}) copy-start(f32[2,4]{1,0:T(2,128)} %get-tuple-element.49) | copy-start | bytes 100
  72.0 10.2 %all-to-all-start = ((f32[4,1,16384]{2,1,0:T(1,128)}), f32[4,1,16384]{2,1,0:T(1,128)S(1)}, u32[]{:S(2)}, u32[]{:S(2)}) async-start(f32[4,1,16384]{2,1,0:T(1,128)} %reshape.274), calls=%async_computation | async-start | bytes 524288 | tf_op jit(solution)/shard_map/all_to_all | solution.py:136
  75.9 9.8 %copy-start.30 = (pred[4,4]{1,0:T(4,128)(4,1)S(1)}, pred[4,4]{1,0:T(4,128)(4,1)}, u32[]{:S(2)}) copy-start(pred[4,4]{1,0:T(4,128)(4,1)} %iota_compare_fusion.1) | copy-start | bytes 52
  84.3 7.2 %copy-start.28 = (f32[2,4]{1,0:T(2,128)S(1)}, f32[2,4]{1,0:T(2,128)}, u32[]{:S(2)}) copy-start(f32[2,4]{1,0:T(2,128)} %mul.529) | copy-start | bytes 100
  84.3 7.4 %copy-start.24 = (bf16[2,32,1,1]{1,0,2,3:T(2,128)(2,1)S(1)}, bf16[2,32,1,1]{1,0,2,3:T(2,128)(2,1)}, u32[]{:S(2)}) copy-start(bf16[2,32,1,1]{1,0,2,3:T(2,128)(2,1)} %fusion.81) | copy-start | bytes 388
  85.7 18.4 %copy-start.29 = (f32[2,4]{1,0:T(2,128)S(1)}, f32[2,4]{1,0:T(2,128)}, u32[]{:S(2)}) copy-start(f32[2,4]{1,0:T(2,128)} %mul.552) | copy-start | bytes 100
  88.1 18.8 %all-to-all-start.1 = ((f32[4,1,16384]{2,1,0:T(1,128)}), f32[4,1,16384]{2,1,0:T(1,128)S(1)}, u32[]{:S(2)}, u32[]{:S(2)}) async-start(f32[4,1,16384]{2,1,0:T(1,128)} %reshape.276), calls=%async_computation.1 | async-start | bytes 524288 | tf_op jit(solution)/shard_map/all_to_all | solution.py:147
  91.5 17.9 %copy-start.31 = (f32[4]{0:T(128)S(1)}, f32[4]{0:T(128)}, u32[]{:S(2)}) copy-start(f32[4]{0:T(128)} %pad.6.clone) | copy-start | bytes 52
  113.5 3.5 %copy-start.2 = (bf16[512,512]{1,0:T(8,128)(2,1)S(1)}, bf16[512,512]{1,0:T(8,128)(2,1)}, u32[]{:S(2)}) copy-start(bf16[512,512]{1,0:T(8,128)(2,1)} %copy-done.1) | copy-start | bytes 1572868
  113.5 3.5 %copy-start.25 = (f32[512]{0:T(512)S(1)}, f32[512]{0:T(512)}, u32[]{:S(2)}) copy-start(f32[512]{0:T(512)} %mul.510) | copy-start | bytes 6148
  (7 other events, 8.8 us)
where the time goes:
time: 127 us; the launch traced here: 126 us
  blocking collectives  30.3 us (24%)
  local copies, waits for them, and re-layouts  28.8 us (23%)
  matrix products  22.6 us (18%)
  other arithmetic  20.4 us (16%)
  starting transfers between devices  19.8 us (16%)
  waiting for transfers between devices  3.3 us (3%)
    ppermute x3, starting transfers between devices, passed_along(): return lax.ppermute(block, axis, route)  12.8 us
    dot_general x8, matrix products, project(): jnp.dot(operand, weights, preferred_element_type=jnp.float32)  12.6 us
    psum x1, blocking collectives, on_device(): reading = lax.psum(partial_value, 'sp')  12.2 us
    psum x1, blocking collectives, from_root(): return lax.psum(kept, axis)  10.5 us
    all_gather x1, blocking collectives, on_device(): lax.all_gather(shard_fading_factor[None], 'sp', axis=0, tiled=True)  7.58 us
    unnamed x75, local copies, waits for them, and re-layouts  6.63 us
    reshape x2, local copies, waits for them, and re-layouts, on_device(): (inner_part + carried_part).reshape(row_count, head_count, HEAD)  5.28 us
    all_to_all x1, starting transfers between devices, on_device(): lax.all_to_all(running[None], 'sp', split_axis=1, concat_axis=0, tiled=True)  3.58 us
  transfers between devices with their start and end apart: 5, of which 1 were waited for; matrix products, arithmetic and copies ran while one was open for 26% of the time, Pallas kernels for 0%

commit v1 on v0

--- a/solution.py
+++ b/solution.py
@@ -8,6 +8,15 @@
 CONV = 4
 BLOCK = 128
 epsilon = 1e-06
+
+
+def doubling_sum(shard, axis):
+    n_dev = lax.axis_size(axis)
+    summed, hop = (shard, 1)
+    while hop < n_dev:
+        summed = summed + lax.ppermute(summed, axis, [(i, i ^ hop) for i in range(n_dev)])
+        hop = 2 * hop
+    return summed
 
 
 def passed_along(block, axis, distance):
@@ -197,7 +206,7 @@
     stored_portion = lax.dynamic_slice_in_dim(write_now, row_start, local_count, 1)
     read_part = lax.dynamic_slice_in_dim(read_now, row_start, local_count, 1)
     partial_value = read_new(cache_rows, stored_portion, read_part, new_decay, step_now, value_now)
-    reading = lax.psum(partial_value, "sp")
+    reading = doubling_sum(partial_value, "sp")
     new_mixed = reading + own_skip.reshape(group_count, per_group)[:, :, None] * value_now
     new_gated = new_mixed.reshape(1, channels) * jax.nn.silu(new_gate.astype(jnp.float32))
     step_whole = (group_norm(new_gated, group_count) * own_gain).astype(jnp.bfloat16)[0]

time: 127 us -> 126 us (level)
  blocking collectives: 30.3 us -> 18.1 us
  waiting for transfers between devices: 3.3 us -> 7.27 us
  starting transfers between devices: 19.8 us -> 23.6 us
  other arithmetic: 20.4 us -> 22.8 us
    psum x1 -> x0, blocking collectives: 12.2 us -> none  [on_device(): reading = lax.psum(partial_value, 'sp')]
    all_to_all x1, waiting for transfers between devices: 0.01 us -> 3.8 us  [on_device(): lax.all_to_all(prefix_rows, 'sp', split_axis=0, concat_axis=1, tiled=True)]
    ppermute x0 -> x2, starting transfers between devices: none -> 2.86 us  [doubling_sum(): lax.ppermute(summed, axis, [(i, i ^ hop) for i in range(n_dev)])]
    unnamed x75 -> x73, local copies, waits for them, and re-layouts: 6.63 us -> 6.56 us
  transfers between devices with their start and end apart: 5 -> 7, of which waited for: 1 -> 2; matrix products, arithmetic and copies ran while one was open for 26% -> 28% of each run, Pallas kernels for 0% -> 0%
where the time goes in v1:
time: 126 us; the launch traced here: 125 us
  local copies, waits for them, and re-layouts  29.2 us (23%)
  starting transfers between devices  23.6 us (19%)
  matrix products  23.1 us (18%)
  other arithmetic  22.8 us (18%)
  blocking collectives  18.1 us (14%)
  waiting for transfers between devices  7.27 us (6%)
    ppermute x3, starting transfers between devices, passed_along(): return lax.ppermute(block, axis, route)  12.8 us
    dot_general x8, matrix products, project(): jnp.dot(operand, weights, preferred_element_type=jnp.float32)  12.6 us
    psum x1, blocking collectives, from_root(): return lax.psum(kept, axis)  10.5 us
    all_gather x1, blocking collectives, on_device(): lax.all_gather(shard_fading_factor[None], 'sp', axis=0, tiled=True)  7.58 us
    unnamed x73, local copies, waits for them, and re-layouts  6.56 us
    reshape x2, local copies, waits for them, and re-layouts, on_device(): (inner_part + carried_part).reshape(row_count, head_count, HEAD)  5.27 us
    all_to_all x1, starting transfers between devices, on_device(): lax.all_to_all(running[None], 'sp', split_axis=1, concat_axis=0, tiled=True)  4.24 us
    all_to_all x1, waiting for transfers between devices, on_device(): lax.all_to_all(prefix_rows, 'sp', split_axis=0, concat_axis=1, tiled=True)  3.8 us
  transfers between devices with their start and end apart: 7, of which 2 were waited for; matrix products, arithmetic and copies ran while one was open for 28% of the time, Pallas kernels for 0%

profile of v1, /device:TPU:0, one launch (start us, length us, event | category | flops | bytes accessed | tf_op | source)
XLA Modules:
  0.0 125.4 jit_solution(8295340781273835069)
XLA Ops:
  0.7 1.6 %copy-done = bf16[512,2048]{1,0:T(8,128)(2,1)S(1)} copy-done((bf16[512,2048]{1,0:T(8,128)(2,1)S(1)}, bf16[512,2048]{1,0:T(8,128)(2,1)}, u32[]{:S(2)}) %copy-start) | copy-done | bytes 2097176
  2.2 1.9 %convolution_convert_fusion.2 = bf16[512,256]{1,0:T(8,128)(2,1)S(1)} fusion(bf16[512,2048]{1,0:T(8,128)(2,1)S(1)} %copy-done, bf16[2048,256]{1,0:T(8,128)(2,1)} %param.18), kind=kOutput, calls=%fused_computation.11 | convolution fusion | flops 537001984 | bytes 3407872 | tf_op jit(solution)/shard_map/dot_general | solution.py:34
  4.8 5.7 %collective-permute-start.2 = (bf16[3,256]{1,0:T(4,128)(2,1)}, bf16[3,256]{1,0:T(4,128)(2,1)}, u32[]{:S(2)}, u32[]{:S(2)}) collective-permute-start(bf16[3,256]{1,0:T(4,128)(2,1)} %get-tuple-element.57), channel_id=1, source_target_pairs={{0,4},{4,8},{8,12},{1,5},{5,9},{9,13},{2,6},{6,10},{10,14},{3,7},{... | collective-permute-start | bytes 4616 | tf_op jit(solution)/shard_map/ppermute | solution.py:25
  11.8 3.6 %collective-permute-start.1 = (bf16[3,256]{1,0:T(4,128)(2,1)}, bf16[3,256]{1,0:T(4,128)(2,1)}, u32[]{:S(2)}, u32[]{:S(2)}) collective-permute-start(bf16[3,256]{1,0:T(4,128)(2,1)} %get-tuple-element.54), channel_id=1, source_target_pairs={{0,4},{4,8},{8,12},{1,5},{5,9},{9,13},{2,6},{6,10},{10,14},{3,7},{... | collective-permute-start | bytes 4616 | tf_op jit(solution)/shard_map/ppermute | solution.py:25
  15.4 1.3 %convolution_convert_fusion.1 = bf16[512,512]{1,0:T(8,128)(2,1)S(1)} fusion(bf16[512,2048]{1,0:T(8,128)(2,1)S(1)} %copy-done, bf16[2048,512]{1,0:T(8,128)(2,1)S(1)} %copy-done.3), kind=kOutput, calls=%fused_computation.9 | convolution fusion | flops 1074003968 | bytes 4718592 | tf_op jit(solution)/shard_map/dot_general | solution.py:34
  18.1 3.5 %collective-permute-start = (bf16[3,512]{1,0:T(4,128)(2,1)}, bf16[3,512]{1,0:T(4,128)(2,1)}, u32[]{:S(2)}, u32[]{:S(2)}) collective-permute-start(bf16[3,512]{1,0:T(4,128)(2,1)} %get-tuple-element.52), channel_id=1, source_target_pairs={{0,4},{4,8},{8,12},{1,5},{5,9},{9,13},{2,6},{6,10},{10,14},{3,7},{... | collective-permute-start | bytes 9224 | tf_op jit(solution)/shard_map/ppermute | solution.py:25
  22.4 1.5 %fusion.96 = f32[1,256]{1,0:T(1,128)S(1)} fusion(bf16[2048,1]{0,1:T(2,128)(2,1)S(1)} %reshape.251, bf16[2048,256]{1,0:T(8,128)(2,1)} %param.19), kind=kOutput, calls=%fused_computation.194 | convolution fusion | flops 1048576 | bytes 1053696 | tf_op jit(solution)/shard_map/dot_general | solution.py:34
  26.5 2.0 %fusion.99 = f32[1,512]{1,0:T(1,128)S(1)} fusion(bf16[2048,1]{0,1:T(2,128)(2,1)S(1)} %reshape.251, bf16[2048,512]{1,0:T(8,128)(2,1)} %param.20), kind=kOutput, calls=%fused_computation.197 | convolution fusion | flops 2097152 | bytes 2103296 | tf_op jit(solution)/shard_map/dot_general | solution.py:34
  28.5 7.6 %all-gather.1 = f32[4,2,4]{2,1,0:T(2,128)S(1)} all-gather(f32[1,2,4]{2,1,0:T(2,128)S(1)} %bitcast.153), channel_id=2, replica_groups=mesh['grp'=2,'sp'=4,'tp'=4] {'sp'}, dimensions={0}, use_global_device_ids=true | all-gather | bytes 160 | tf_op jit(solution)/shard_map/all_gather | solution.py:141
  36.2 10.5 %all-reduce = (bf16[3,512]{1,0:T(4,128)(2,1)S(1)}, bf16[3,256]{1,0:T(4,128)(2,1)S(1)}, bf16[3,256]{1,0:T(4,128)(2,1)S(1)}) all-reduce(bf16[3,512]{1,0:T(4,128)(2,1)S(1)} %get-tuple-element.53, bf16[3,256]{1,0:T(4,128)(2,1)S(1)} %get-tuple-element.56, ...), channel_id=1, replica_groups=mesh['grp'=2,'sp'=4,'tp'=4] {'sp'}, use_global_device_ids=true, to_apply=%region_7.8 | all-reduce | flops 3072 | bytes 12288 | tf_op jit(solution)/shard_map/psum | solution.py:30
  49.4 2.4 %fusion.90 = (f32[4,128,2,4]{3,2,1,0:T(2,128)}, f32[4,128,2,4]{3,2,1,0:T(2,128)S(1)}) fusion(f32[4,128,2,4]{3,2,1,0:T(2,128)S(1)} %fusion.94, f32[4,128,2,4]{3,2,1,0:T(2,128)} %copy.149, f32[4,2,4]{2,1,0:T(2,128)S(1)} %get-tuple-element.47), kind=kLoop, calls=%fused_computation.187 | loop fusion | flops 8192 | bytes 65664 | tf_op jit(solution)/shard_map/exp | solution.py:173
  55.7 1.2 copy.148
  61.8 1.3 %multiply_convert_fusion.4 = bf16[512,512]{1,0:T(8,128)(2,1)S(1)} fusion(f32[515,512]{1,0:T(8,128)S(1)} %maximum_convert_fusion, f32[512]{0:T(512)} %bitcast.142, f32[512]{0:T(512)} %bitcast.141, f32[512]{0:T(512)} %bitcast.140, f32[512]{0:T(512)} %bitcast.139), kind=kLoop, calls=%fused_computation.44 | loop fusion | flops 3145728 | bytes 4726784 | tf_op jit(solution)/shard_map/convert_element_type | solution.py:112
  64.1 2.0 %reshape.229 = bf16[4,128,2,4,64]{1,0,4,3,2:T(4,128)(2,1)} reshape(bf16[512,512]{0,1:T(8,128)(2,1)} %copy.140) | data formatting | bytes 1048576 | tf_op jit(solution)/shard_map/reshape | solution.py:118
  66.1 1.3 %multiply_convert_fusion.3 = bf16[4,128,2,4,64]{1,0,4,3,2:T(4,128)(2,1)S(1)} fusion(bf16[4,128,2,4,64]{1,0,4,3,2:T(4,128)(2,1)} %reshape.229, f32[4,128,2,4]{1,0,3,2:T(4,128)S(1)} %copy.150), kind=kLoop, calls=%fused_computation.38 | loop fusion | flops 786432 | bytes 1064960 | tf_op jit(solution)/shard_map/convert_element_type | solution.py:127
  68.8 1.2 copy.153
  71.2 4.2 %all-to-all-start = ((f32[4,1,16384]{2,1,0:T(1,128)}), f32[4,1,16384]{2,1,0:T(1,128)}, u32[]{:S(2)}, u32[]{:S(2)}) async-start(f32[4,1,16384]{2,1,0:T(1,128)} %reshape.274), calls=%async_computation | async-start | bytes 524288 | tf_op jit(solution)/shard_map/all_to_all | solution.py:145
  78.7 3.5 %all-to-all-done = f32[4,1,16384]{2,1,0:T(1,128)} async-done(((f32[4,1,16384]{2,1,0:T(1,128)}), f32[4,1,16384]{2,1,0:T(1,128)}, u32[]{:S(2)}, u32[]{:S(2)}) %all-to-all-start) | async-done | bytes 262176 | tf_op jit(solution)/shard_map/all_to_all | solution.py:145
  82.7 2.3 %reduce.9 = f32[4,16384]{1,0:T(4,128)S(1)} reduce(f32[4,1,16384]{2,1,0:T(1,128)} %all-to-all-done, f32[]{:T(128)} %broadcast.118), dimensions={1}, to_apply=%all_to_all.6.reduce_sub_computation | reduce | bytes 524292 | tf_op jit(solution)/shard_map/all_to_all | solution.py:145
  85.3 1.3 %fusion.35 = bf16[2,4,1,32,64]{4,2,3,1,0:T(2,128)(2,1)S(1)} fusion(f32[4,2,4,1,1]{0,3,4,2,1:T(1,128)S(1)} %copy.173, f32[4,32,2,4,64]{4,3,2,1,0:T(4,128)S(1)} %bitcast.123), kind=kOutput, calls=%fused_computation.69 | convolution fusion | flops 786432 | bytes 295040 | tf_op jit(solution)/shard_map/kge,kngep->ngep/dot_general | solution.py:153
  87.0 1.5 %collective-permute-start.3 = (f32[2,4,64]{2,1,0:T(4,128)S(1)}, f32[2,4,64]{2,1,0:T(4,128)S(1)}, u32[]{:S(2)}, u32[]{:S(2)}) collective-permute-start(f32[2,4,64]{2,1,0:T(4,128)S(1)} %bitcast.137), channel_id=1, source_target_pairs={{0,4},{4,0},{8,12},{12,8},{1,5},{5,1},{9,13},{13,9},{2,6},{6,2},{1... | collective-permute-start | bytes 6152 | tf_op jit(solution)/shard_map/ppermute | solution.py:17
  88.5 3.1 %convolution_bitcast_fusion.2 = f32[4,128,2,4,64]{1,4,3,2,0:T(8,128)} fusion(f32[4,2,4,128]{3,2,1,0:T(4,128)S(1)} %copy.146, f32[4,2,4,128]{3,2,1,0:T(4,128)S(1)} %copy.144, f32[4,2,128,128]{3,2,1,0:T(8,128)} %fusion.40, pred[128,128]{1,0:T(8,128)(4,1)S(1)} %iota_compare_fusion, bf16[4,128,2,4,64]{1,0,4,3,2:T(4,128)(2,1)} %reshape.229), kind=kOutput, calls=%fused_computation.5 | convolution fusion | flops 69730304 | bytes 2146304 | tf_op jit(solution)/shard_map/bgels,bsgep->blgep/dot_general | solution.py:169
  91.7 1.3 %collective-permute-start.4 = (f32[2,4,64]{2,1,0:T(4,128)S(1)}, f32[2,4,64]{2,1,0:T(4,128)S(1)}, u32[]{:S(2)}, u32[]{:S(2)}) collective-permute-start(f32[2,4,64]{2,1,0:T(4,128)S(1)} %add.240), channel_id=1, source_target_pairs={{0,8},{4,12},{8,0},{12,4},{1,9},{5,13},{9,1},{13,5},{2,10},{6,14},... | collective-permute-start | bytes 6152 | tf_op jit(solution)/shard_map/ppermute | solution.py:17
  93.0 1.3 %convolution_bitcast_fusion.3 = f32[4,32,2,4,64]{4,0,1,3,2:T(4,128)S(1)} fusion(f32[4,32,2,4,64]{4,3,2,1,0:T(4,128)S(1)} %bitcast.124, f32[4,2,4]{0,2,1:T(4,128)S(1)} %copy.156, f32[4,2,4]{0,2,1:T(4,128)S(1)} %copy.155, pred[4,4]{1,0:T(4,128)(4,1)S(1)} %copy-done.28), kind=kOutput, calls=%fused_computation.10 | convolution fusion | flops 3145984 | bytes 524560 | tf_op jit(solution)/shard_map/jkge,kngep->jngep/dot_general | solution.py:149
  95.5 3.8 %all-to-all-start.1 = ((f32[4,1,16384]{2,1,0:T(1,128)}), f32[4,1,16384]{2,1,0:T(1,128)S(1)}, u32[]{:S(2)}, u32[]{:S(2)}) async-start(f32[4,1,16384]{2,1,0:T(1,128)} %reshape.276), calls=%async_computation.1 | async-start | bytes 524288 | tf_op jit(solution)/shard_map/all_to_all | solution.py:156
  102.0 3.8 %all-to-all-done.1 = f32[4,1,16384]{2,1,0:T(1,128)S(1)} async-done(((f32[4,1,16384]{2,1,0:T(1,128)}), f32[4,1,16384]{2,1,0:T(1,128)S(1)}, u32[]{:S(2)}, u32[]{:S(2)}) %all-to-all-start.1) | async-done | bytes 262176 | tf_op jit(solution)/shard_map/all_to_all | solution.py:156
  105.8 1.3 %reduce.10 = f32[4,16384]{1,0:T(4,128)S(1)} reduce(f32[4,1,16384]{2,1,0:T(1,128)S(1)} %all-to-all-done.1, f32[]{:T(128)} %broadcast.118), dimensions={1}, to_apply=%all_to_all.8.reduce_sub_computation | reduce | bytes 524292 | tf_op jit(solution)/shard_map/all_to_all | solution.py:156
  108.4 2.3 %fusion.1 = f32[4,128,2,4,64]{1,4,3,2,0:T(8,128)S(1)} fusion(f32[4,128,2,4,64]{1,4,3,2,0:T(8,128)} %convolution_bitcast_fusion.2, f32[1,128,2,4,64]{1,4,3,2,0:T(8,128)} %get-tuple-element.41, f32[1,128,2,4,64]{1,4,3,2,0:T(8,128)} %get-tuple-element.42, f32[1,128,2,4,64]{1,4,3,2,0:T(8,128)} %get-tuple-element.43, f32[4]{0:T(128)S(1)} %copy-done.29, ...), kind=kOutput, calls=%fused_computation.4 | convolution fusion | flops 404488192 | bytes 3424400 | tf_op jit(solution)/shard_map/blgn,bngep->blgep/dot_general | solution.py:173
  110.7 1.8 %copy.184 = f32[4,128,2,4,64]{4,3,2,1,0:T(4,128)} copy(f32[4,128,2,4,64]{1,4,3,2,0:T(8,128)S(1)} %fusion.1) | data formatting | bytes 2097152 | tf_op jit(solution)/shard_map/reshape | solution.py:179
  112.5 3.5 %reshape.263 = f32[512,512]{1,0:T(8,128)} reshape(f32[4,128,2,4,64]{4,3,2,1,0:T(4,128)} %copy.184) | data formatting | bytes 2097152 | tf_op jit(solution)/shard_map/reshape | solution.py:179
  116.0 4.6 %fusion.93 = (f32[512,512]{1,0:T(8,128)}, f32[512,512]{1,0:T(8,128)}) fusion(bf16[512,2048]{1,0:T(8,128)(2,1)S(1)} %copy-done, bf16[2048,512]{1,0:T(8,128)(2,1)} %param.20, f32[512,512]{1,0:T(8,128)} %reshape.263, bf16[512,512]{1,0:T(8,128)(2,1)S(1)} %copy-done.2, f32[512]{0:T(512)S(1)} %copy-done.23), kind=kOutput, calls=%fused_computation.190 | convolution fusion | flops 1076625408 | bytes 7866368 | tf_op jit(solution)/shard_map/dot_general | solution.py:34
  120.6 1.9 %mul.516 = f32[512,2,256]{2,1,0:T(2,128)S(1)} reshape(f32[512,512]{1,0:T(8,128)} %get-tuple-element.63) | data formatting | bytes 2097152 | tf_op jit(solution)/shard_map/mul | solution.py:48
  (162 shorter events, 34.1 us)
Async XLA Ops:
  0.6 9.8 %copy-start.6 = (bf16[2048,256]{1,0:T(8,128)(2,1)S(1)}, bf16[2048,256]{1,0:T(8,128)(2,1)}, u32[]{:S(2)}) copy-start(bf16[2048,256]{1,0:T(8,128)(2,1)} %param.19) | copy-start | bytes 3145732
  4.2 7.6 %copy-start.9 = (bf16[512,256]{1,0:T(8,128)(2,1)}, bf16[512,256]{1,0:T(8,128)(2,1)S(1)}, u32[]{:S(2)}) copy-start(bf16[512,256]{1,0:T(8,128)(2,1)S(1)} %convolution_convert_fusion.2) | copy-start | bytes 786436
  4.2 11.2 %copy-start.3 = (bf16[2048,512]{1,0:T(8,128)(2,1)S(1)}, bf16[2048,512]{1,0:T(8,128)(2,1)}, u32[]{:S(2)}) copy-start(bf16[2048,512]{1,0:T(8,128)(2,1)} %param.17) | copy-start | bytes 6291460
  4.8 52.9 %collective-permute-start.2 = (bf16[3,256]{1,0:T(4,128)(2,1)}, bf16[3,256]{1,0:T(4,128)(2,1)}, u32[]{:S(2)}, u32[]{:S(2)}) collective-permute-start(bf16[3,256]{1,0:T(4,128)(2,1)} %get-tuple-element.57), channel_id=1, source_target_pairs={{0,4},{4,8},{8,12},{1,5},{5,9},{9,13},{2,6},{6,10},{10,14},{3,7},{... | collective-permute-start | bytes 4616 | tf_op jit(solution)/shard_map/ppermute | solution.py:25
  11.8 10.3 %copy-start.21 = (bf16[2048]{0:T(1024)(128)(2,1)S(1)}, bf16[2048]{0:T(1024)(128)(2,1)}, u32[]{:S(2)}) copy-start(bf16[2048]{0:T(1024)(128)(2,1)} %param.16) | copy-start | bytes 12292
  11.8 10.3 %copy-start.5 = (bf16[2048,256]{1,0:T(8,128)(2,1)S(1)}, bf16[2048,256]{1,0:T(8,128)(2,1)}, u32[]{:S(2)}) copy-start(bf16[2048,256]{1,0:T(8,128)(2,1)} %param.18) | copy-start | bytes 3145732
  11.8 48.0 %collective-permute-start.1 = (bf16[3,256]{1,0:T(4,128)(2,1)}, bf16[3,256]{1,0:T(4,128)(2,1)}, u32[]{:S(2)}, u32[]{:S(2)}) collective-permute-start(bf16[3,256]{1,0:T(4,128)(2,1)} %get-tuple-element.54), channel_id=1, source_target_pairs={{0,4},{4,8},{8,12},{1,5},{5,9},{9,13},{2,6},{6,10},{10,14},{3,7},{... | collective-permute-start | bytes 4616 | tf_op jit(solution)/shard_map/ppermute | solution.py:25
  18.1 42.5 %collective-permute-start = (bf16[3,512]{1,0:T(4,128)(2,1)}, bf16[3,512]{1,0:T(4,128)(2,1)}, u32[]{:S(2)}, u32[]{:S(2)}) collective-permute-start(bf16[3,512]{1,0:T(4,128)(2,1)} %get-tuple-element.52), channel_id=1, source_target_pairs={{0,4},{4,8},{8,12},{1,5},{5,9},{9,13},{2,6},{6,10},{10,14},{3,7},{... | collective-permute-start | bytes 9224 | tf_op jit(solution)/shard_map/ppermute | solution.py:25
  21.6 2.3 %copy-start.4 = (bf16[2048,512]{1,0:T(8,128)(2,1)S(1)}, bf16[2048,512]{1,0:T(8,128)(2,1)}, u32[]{:S(2)}) copy-start(bf16[2048,512]{1,0:T(8,128)(2,1)} %param.17) | copy-start | bytes 6291460
  22.1 2.2 %copy-start.31 = (f32[32]{0:T(128)S(1)}, f32[32]{0:T(128)}, u32[]{:S(2)}) copy-start(f32[32]{0:T(128)} %param.26) | copy-start | bytes 388
  22.1 2.3 %copy-start.30 = (f32[32]{0:T(128)S(1)}, f32[32]{0:T(128)}, u32[]{:S(2)}) copy-start(f32[32]{0:T(128)} %param.25) | copy-start | bytes 388
  22.1 2.4 %copy-start.10 = (f32[512,8]{0,1:T(8,128)S(1)}, f32[512,8]{0,1:T(8,128)}, u32[]{:S(2)}) copy-start(f32[512,8]{0,1:T(8,128)} %param.27) | copy-start | bytes 49156
  25.2 21.5 %copy-start.24 = (bf16[4,1024]{1,0:T(4,128)(2,1)S(1)}, bf16[4,1024]{1,0:T(4,128)(2,1)}, u32[]{:S(2)}) copy-start(bf16[4,1024]{1,0:T(4,128)(2,1)} %param.23) | copy-start | bytes 24580
  25.5 23.0 %copy-start.25 = (bf16[4,1024]{1,0:T(4,128)(2,1)S(1)}, bf16[4,1024]{1,0:T(4,128)(2,1)}, u32[]{:S(2)}) copy-start(bf16[4,1024]{1,0:T(4,128)(2,1)} %param.24) | copy-start | bytes 24580
  26.5 25.3 %copy-start.20 = (bf16[4,2048]{1,0:T(4,128)(2,1)S(1)}, bf16[4,2048]{1,0:T(4,128)(2,1)}, u32[]{:S(2)}) copy-start(bf16[4,2048]{1,0:T(4,128)(2,1)} %param.22) | copy-start | bytes 49156
  26.5 26.6 %copy-start.32 = (f32[32]{0:T(128)S(1)}, f32[32]{0:T(128)}, u32[]{:S(2)}) copy-start(f32[32]{0:T(128)} %param.28) | copy-start | bytes 388
  63.1 4.6 %copy-start.1 = (bf16[512,512]{1,0:T(8,128)(2,1)}, bf16[512,512]{1,0:T(8,128)(2,1)S(1)}, u32[]{:S(2)}) copy-start(bf16[512,512]{1,0:T(8,128)(2,1)S(1)} %multiply_convert_fusion.4) | copy-start | bytes 1572868
  67.7 7.7 %copy-start.16 = (f32[1,256]{1,0:T(1,128)S(1)}, f32[1,256]{1,0:T(1,128)}, u32[]{:S(2)}) copy-start(f32[1,256]{1,0:T(1,128)} %get-tuple-element.24) | copy-start | bytes 3076
  67.7 7.7 %copy-start.17 = (f32[1,256]{1,0:T(1,128)S(1)}, f32[1,256]{1,0:T(1,128)}, u32[]{:S(2)}) copy-start(f32[1,256]{1,0:T(1,128)} %get-tuple-element.25) | copy-start | bytes 3076
  67.7 7.7 %copy-start.18 = (f32[1,256]{1,0:T(1,128)S(1)}, f32[1,256]{1,0:T(1,128)}, u32[]{:S(2)}) copy-start(f32[1,256]{1,0:T(1,128)} %get-tuple-element.26) | copy-start | bytes 3076
  67.7 7.7 %copy-start.19 = (f32[1,256]{1,0:T(1,128)S(1)}, f32[1,256]{1,0:T(1,128)}, u32[]{:S(2)}) copy-start(f32[1,256]{1,0:T(1,128)} %get-tuple-element.27) | copy-start | bytes 3076
  71.2 10.9 %all-to-all-start = ((f32[4,1,16384]{2,1,0:T(1,128)}), f32[4,1,16384]{2,1,0:T(1,128)}, u32[]{:S(2)}, u32[]{:S(2)}) async-start(f32[4,1,16384]{2,1,0:T(1,128)} %reshape.274), calls=%async_computation | async-start | bytes 524288 | tf_op jit(solution)/shard_map/all_to_all | solution.py:145
  76.5 10.1 %copy-start.26 = (f32[2,4]{1,0:T(2,128)S(1)}, f32[2,4]{1,0:T(2,128)}, u32[]{:S(2)}) copy-start(f32[2,4]{1,0:T(2,128)} %mul.529) | copy-start | bytes 100
  76.5 10.3 %copy-start.22 = (bf16[2,32,1,1]{1,0,2,3:T(2,128)(2,1)S(1)}, bf16[2,32,1,1]{1,0,2,3:T(2,128)(2,1)}, u32[]{:S(2)}) copy-start(bf16[2,32,1,1]{1,0,2,3:T(2,128)(2,1)} %fusion.81) | copy-start | bytes 388
  86.8 6.2 %copy-start.28 = (pred[4,4]{1,0:T(4,128)(4,1)S(1)}, pred[4,4]{1,0:T(4,128)(4,1)}, u32[]{:S(2)}) copy-start(pred[4,4]{1,0:T(4,128)(4,1)} %iota_compare_fusion.1) | copy-start | bytes 52
  87.0 4.7 %collective-permute-start.3 = (f32[2,4,64]{2,1,0:T(4,128)S(1)}, f32[2,4,64]{2,1,0:T(4,128)S(1)}, u32[]{:S(2)}, u32[]{:S(2)}) collective-permute-start(f32[2,4,64]{2,1,0:T(4,128)S(1)} %bitcast.137), channel_id=1, source_target_pairs={{0,4},{4,0},{8,12},{12,8},{1,5},{5,1},{9,13},{13,9},{2,6},{6,2},{1... | collective-permute-start | bytes 6152 | tf_op jit(solution)/shard_map/ppermute | solution.py:17
  91.7 8.4 %copy-start.27 = (f32[2,4]{1,0:T(2,128)S(1)}, f32[2,4]{1,0:T(2,128)}, u32[]{:S(2)}) copy-start(f32[2,4]{1,0:T(2,128)} %mul.552) | copy-start | bytes 100
  91.7 8.4 %collective-permute-start.4 = (f32[2,4,64]{2,1,0:T(4,128)S(1)}, f32[2,4,64]{2,1,0:T(4,128)S(1)}, u32[]{:S(2)}, u32[]{:S(2)}) collective-permute-start(f32[2,4,64]{2,1,0:T(4,128)S(1)} %add.240), channel_id=1, source_target_pairs={{0,8},{4,12},{8,0},{12,4},{1,9},{5,13},{9,1},{13,5},{2,10},{6,14},... | collective-permute-start | bytes 6152 | tf_op jit(solution)/shard_map/ppermute | solution.py:17
  95.5 12.9 %copy-start.29 = (f32[4]{0:T(128)S(1)}, f32[4]{0:T(128)}, u32[]{:S(2)}) copy-start(f32[4]{0:T(128)} %pad.6.clone) | copy-start | bytes 52
  95.5 10.3 %all-to-all-start.1 = ((f32[4,1,16384]{2,1,0:T(1,128)}), f32[4,1,16384]{2,1,0:T(1,128)S(1)}, u32[]{:S(2)}, u32[]{:S(2)}) async-start(f32[4,1,16384]{2,1,0:T(1,128)} %reshape.276), calls=%async_computation.1 | async-start | bytes 524288 | tf_op jit(solution)/shard_map/all_to_all | solution.py:156
  112.5 3.5 %copy-start.2 = (bf16[512,512]{1,0:T(8,128)(2,1)S(1)}, bf16[512,512]{1,0:T(8,128)(2,1)}, u32[]{:S(2)}) copy-start(bf16[512,512]{1,0:T(8,128)(2,1)} %copy-done.1) | copy-start | bytes 1572868
  112.5 3.5 %copy-start.23 = (f32[512]{0:T(512)S(1)}, f32[512]{0:T(512)}, u32[]{:S(2)}) copy-start(f32[512]{0:T(512)} %mul.510) | copy-start | bytes 6148
  (8 other events, 12.0 us)
